TPU v7x, 32 devices: a whole 2x2x4 slice. The times are simulated.
32 devices in a mesh: sp: 32 (over z, y, x, core), fs: 1, tp: 1.
Axes of the slice: x: 2, y: 2, z: 4, core: 2. Of those that a mesh axis runs over, the one named last changes fastest.
Arguments:
- tokens: bfloat16 [4096, 2048], P(('fs', 'sp'), 'tp'), may hold values from -450 to 450
- documents: int32 [4096], P(('fs', 'sp')), may hold values from 0 to 3, never falling along the last dimension, each value on 1 to 2048 neighbouring positions
- norm_gain: bfloat16 [2048], P('tp'), may hold values from 0.099609375 to 1.8984375
- out_gate_weight: bfloat16 [2048, 1024], P('sp', 'tp'), may hold values from -0.125 to 0.125
- in_gate_weight: bfloat16 [2048, 1024], P('sp', 'tp'), may hold values from -0.125 to 0.125
- value_weight: bfloat16 [2048, 1024], P('sp', 'tp'), may hold values from -0.125 to 0.125
- conv_taps: bfloat16 [3, 1024], P(None, 'tp'), may hold values from -3.5 to 3.5
- state_in_weight: bfloat16 [2048, 1024], P('sp', 'tp'), may hold values from -0.125 to 0.125
- decay_rate: float32 [64, 64], P('tp'), may hold values from 4e-05 to 2.01
- frequency: float32 [64, 64], P('tp'), may hold values from 0 to 32
- step_log: float32 [64], P('tp'), may hold values from -3.9121 to -1.6094
- input_real: float32 [64, 64, 16], P('tp'), may hold values from -1 to 1
- input_imag: float32 [64, 64, 16], P('tp'), may hold values from -1 to 1
- readout_real: float32 [64, 16, 64], P('tp'), may hold values from -0.75 to 0.75
- readout_imag: float32 [64, 16, 64], P('tp'), may hold values from -0.75 to 0.75
- skip_gain: float32 [1024], P('tp'), may hold values from -4 to 4
- conv_out_weight: bfloat16 [1024, 2048], P('tp', 'sp'), may hold values from -0.125 to 0.125
- state_out_weight: bfloat16 [1024, 2048], P('tp', 'sp'), may hold values from -0.125 to 0.125
Outputs:
- mixed: bfloat16 [4096, 2048], P(('fs', 'sp', 'tp'))
All inputs are finite; a program needn't handle non-finite values.
Results may differ from a plain program's by a relative error of at most 0.015.
Values may be sent and summed in bfloat16 or wider, within the bound.
A program may use at most 64 MiB of HBM per device.

v0:
```python
import math

import jax
import jax.numpy as jnp
from jax import lax
from jax.sharding import PartitionSpec as P

D = 2048
TAPS = 3


EPS = 1e-06


def prefix(part, axis, combine, identity):
    place = lax.axis_index(axis)
    gathered = jax.tree.map(lambda a: lax.all_gather(a, axis), part)
    state = jax.tree.map(lambda a, e: jnp.zeros_like(a) + jnp.asarray(e, a.dtype), part, identity)

    def one(turn, state):
        return combine(
            state, jax.tree.map(lambda a: lax.dynamic_index_in_dim(a, turn, 0, False), gathered)
        )

    return lax.fori_loop(0, place, one, state)


def from_behind(block, axis, distance):
    devices = range(lax.axis_size(axis))
    route = [(i - distance, i) for i in devices if i - distance in devices]
    return lax.ppermute(block, axis, route)


def chain_step(earlier, later):
    dec_real, dec_imag, end_real, end_imag, first_doc, last_doc = earlier
    late_dec_real, late_dec_imag, late_end_real, late_end_imag, late_first, late_last = later
    joined = (late_first == last_doc) | (last_doc < 0.0) | (late_first < 0.0)
    link = joined.astype(jnp.float32)
    carried_real = late_dec_real * end_real - late_dec_imag * end_imag
    carried_imag = late_dec_real * end_imag + late_dec_imag * end_real
    return (
        link * (late_dec_real * dec_real - late_dec_imag * dec_imag),
        link * (late_dec_real * dec_imag + late_dec_imag * dec_real),
        late_end_real + link * carried_real,
        late_end_imag + link * carried_imag,
        jnp.where(first_doc < 0.0, late_first, first_doc),
        jnp.where(late_last < 0.0, last_doc, late_last),
    )


def ssm_constants(decay_rate, frequency, step_log, input_real, input_imag):
    step_size = jnp.exp(step_log)[:, None]
    damping = decay_rate * step_size
    turning = frequency * step_size
    fading = jnp.exp(-damping)
    coef_imag = fading * jnp.sin(turning)
    half_sine = jnp.sin(turning / 2.0)
    less_real = jnp.expm1(-damping) * jnp.cos(turning) - 2.0 * half_sine * half_sine
    denominator = decay_rate * decay_rate + frequency * frequency
    ratio_real = (-less_real * decay_rate + coef_imag * frequency) / denominator
    ratio_imag = (-coef_imag * decay_rate - less_real * frequency) / denominator
    bbar_real = ratio_real[..., None] * input_real - ratio_imag[..., None] * input_imag
    bbar_imag = ratio_real[..., None] * input_imag + ratio_imag[..., None] * input_real
    return (bbar_real, bbar_imag, damping.reshape(-1), turning.reshape(-1))


def block_recurrence(
    damping,
    turning,
    bbar_real,
    bbar_imag,
    driven,
    keep_rows,
    doc_rows,
    carry_real,
    carry_imag,
    readout_real,
    readout_imag,
):
    groups, group_size, state_size = readout_real.shape
    row_count = driven.shape[0]
    block = math.gcd(row_count, 16)
    blocks = row_count // block
    steps = jnp.arange(block, dtype=jnp.float32)
    gap = steps[:, None] - steps[None, :]
    lower = (gap >= 0.0).astype(jnp.float32)
    gap_pos = jnp.maximum(gap, 0.0)[:, :, None]
    pair_fade = jnp.exp(-gap_pos * damping[None, None, :])
    pair_real = pair_fade * jnp.cos(gap_pos * turning[None, None, :])
    pair_imag = pair_fade * jnp.sin(gap_pos * turning[None, None, :])
    lead = (steps + 1.0)[:, None]
    lead_fade = jnp.exp(-lead * damping[None, :])
    lead_real = lead_fade * jnp.cos(lead * turning[None, :])
    lead_imag = lead_fade * jnp.sin(lead * turning[None, :])

    def one_block(carry, pieces):
        start_real, start_imag = carry
        inputs, keeps, docs = pieces
        split_rows = inputs.reshape(block, groups, group_size)
        push_real = jnp.einsum(
            "tgh,gph->tgp", split_rows, bbar_real, precision=lax.Precision.HIGHEST
        ).reshape(block, groups * state_size)
        push_imag = jnp.einsum(
            "tgh,gph->tgp", split_rows, bbar_imag, precision=lax.Precision.HIGHEST
        ).reshape(block, groups * state_size)
        same = lower * (docs[:, None] == docs[None, :]).astype(jnp.float32)
        weigh_real = same[:, :, None] * pair_real
        weigh_imag = same[:, :, None] * pair_imag
        alive = (keeps[0] * (docs == docs[0]).astype(jnp.float32))[:, None]
        held_real = jnp.sum(
            weigh_real * push_real[None, :, :] - weigh_imag * push_imag[None, :, :], axis=1
        ) + alive * (lead_real * start_real[None, :] - lead_imag * start_imag[None, :])
        held_imag = jnp.sum(
            weigh_real * push_imag[None, :, :] + weigh_imag * push_real[None, :, :], axis=1
        ) + alive * (lead_real * start_imag[None, :] + lead_imag * start_real[None, :])
        result = jnp.einsum(
            "tgp,ghp->tgh",
            held_real.reshape(block, groups, state_size),
            readout_real,
            precision=lax.Precision.HIGHEST,
        )
        result = result - jnp.einsum(
            "tgp,ghp->tgh",
            held_imag.reshape(block, groups, state_size),
            readout_imag,
            precision=lax.Precision.HIGHEST,
        )
        return ((held_real[-1], held_imag[-1]), result.reshape(block, groups * group_size))

    _, outputs = lax.scan(
        one_block,
        (carry_real, carry_imag),
        (
            driven.reshape(blocks, block, -1),
            keep_rows.reshape(blocks, block),
            doc_rows.reshape(blocks, block),
        ),
    )
    return outputs.reshape(row_count, groups * group_size)


def shards(
    tokens,
    documents,
    norm_gain,
    out_gate_weight,
    in_gate_weight,
    value_weight,
    conv_taps,
    state_in_weight,
    decay_rate,
    frequency,
    step_log,
    input_real,
    input_imag,
    readout_real,
    readout_imag,
    skip_gain,
    conv_out_weight,
    state_out_weight,
):
    row_count = tokens.shape[0]
    groups, state_size = decay_rate.shape
    group_size = input_real.shape[2]
    values = tokens.astype(jnp.float32)
    totals = lax.psum(jnp.sum(values * values, axis=1), "tp")
    scaled = values * lax.rsqrt(totals / D + EPS)[:, None] * norm_gain.astype(jnp.float32)[None, :]
    normed = lax.all_gather(scaled.astype(jnp.bfloat16), "tp", axis=1, tiled=True)
    bbar_real, bbar_imag, damping, turning = ssm_constants(
        decay_rate, frequency, step_log, input_real, input_imag
    )
    doc_float = documents.astype(jnp.float32)
    pieces = (
        lax.all_gather(out_gate_weight, "sp", axis=0, tiled=True),
        lax.all_gather(in_gate_weight, "sp", axis=0, tiled=True),
        lax.all_gather(value_weight, "sp", axis=0, tiled=True),
        lax.all_gather(state_in_weight, "sp", axis=0, tiled=True),
    )
    gate_sum, inner_sum, value_sum, driven_sum = tuple(
        (jnp.dot(normed, piece, preferred_element_type=jnp.float32) for piece in pieces)
    )
    driven_wide = driven_sum.astype(jnp.bfloat16).astype(jnp.float32)
    split_rows = driven_wide.reshape(row_count, groups, group_size)
    backward = (row_count - 1 - jnp.arange(row_count)).astype(jnp.float32)[:, None]
    alive = (documents == documents[-1]).astype(jnp.float32)[:, None]
    fading = jnp.exp(-backward * damping[None, :]) * alive
    weigh_real = (fading * jnp.cos(backward * turning[None, :])).reshape(
        row_count, groups, state_size
    )
    weigh_imag = (fading * jnp.sin(backward * turning[None, :])).reshape(
        row_count, groups, state_size
    )
    moment_real = jnp.einsum(
        "tgp,tgh->gph", weigh_real, split_rows, precision=lax.Precision.HIGHEST
    )
    moment_imag = jnp.einsum(
        "tgp,tgh->gph", weigh_imag, split_rows, precision=lax.Precision.HIGHEST
    )
    end_real = jnp.sum(bbar_real * moment_real - bbar_imag * moment_imag, axis=2).reshape(-1)
    end_imag = jnp.sum(bbar_real * moment_imag + bbar_imag * moment_real, axis=2).reshape(-1)
    whole_doc = (documents[0] == documents[-1]).astype(jnp.float32)
    total_fade = jnp.exp(-row_count * damping) * whole_doc
    element = (
        total_fade * jnp.cos(row_count * turning),
        total_fade * jnp.sin(row_count * turning),
        end_real,
        end_imag,
        doc_float[:1],
        doc_float[-1:],
    )
    identity = (
        jnp.ones_like(end_real),
        jnp.zeros_like(end_real),
        jnp.zeros_like(end_real),
        jnp.zeros_like(end_real),
        jnp.full((1,), -1.0, jnp.float32),
        jnp.full((1,), -1.0, jnp.float32),
    )
    incoming = prefix(element, "sp", chain_step, identity)
    driven_wide, incoming = (driven_wide, incoming)
    out_gate = gate_sum.astype(jnp.bfloat16).astype(jnp.float32)
    in_gate = inner_sum.astype(jnp.bfloat16).astype(jnp.float32)
    value = value_sum.astype(jnp.bfloat16).astype(jnp.float32)
    product = (in_gate * value).astype(jnp.bfloat16)
    margin = TAPS - 1
    tail_same = documents[row_count - margin :] == documents[-1]
    tail_rows = jnp.where(
        tail_same[:, None], product[row_count - margin :], jnp.zeros_like(product[:margin])
    )
    rim_rows = from_behind(tail_rows, "sp", 1)
    in_dec_real, in_dec_imag, in_real, in_imag, in_first, in_last = incoming
    padded = jnp.concatenate([rim_rows, product], axis=0)
    padded_docs = jnp.concatenate([jnp.broadcast_to(in_last, (margin,)), doc_float], axis=0)
    total = jnp.zeros(product.shape, jnp.float32)
    for index in range(TAPS):
        same_doc = (padded_docs[index : index + row_count] == doc_float).astype(jnp.float32)
        total = (
            total
            + conv_taps[index].astype(jnp.float32)[None, :]
            * padded[index : index + row_count].astype(jnp.float32)
            * same_doc[:, None]
        )
    conv_out = (out_gate * total).astype(jnp.bfloat16)
    link_first = (in_last == doc_float[:1]).astype(jnp.float32)
    keep_rows = jnp.concatenate(
        [link_first, (documents[1:] == documents[:-1]).astype(jnp.float32)], axis=0
    )
    readout = block_recurrence(
        damping,
        turning,
        bbar_real,
        bbar_imag,
        driven_wide,
        keep_rows,
        doc_float,
        in_real,
        in_imag,
        readout_real,
        readout_imag,
    )
    ssm_out = jax.nn.gelu(readout + skip_gain[None, :] * driven_wide, approximate=True).astype(
        jnp.bfloat16
    )
    conv_columns, state_columns = (
        lax.all_gather(conv_out_weight, "sp", axis=1, tiled=True),
        lax.all_gather(state_out_weight, "sp", axis=1, tiled=True),
    )
    return lax.psum_scatter(
        (
            jnp.dot(conv_out, conv_columns, preferred_element_type=jnp.float32)
            + jnp.dot(ssm_out, state_columns, preferred_element_type=jnp.float32)
        ).astype(jnp.bfloat16),
        "tp",
        scatter_dimension=0,
        tiled=True,
    )


def solution(mesh):
    placed = (
        P(("fs", "sp"), "tp"),
        P(("fs", "sp")),
        P("tp"),
        P("sp", "tp"),
        P("sp", "tp"),
        P("sp", "tp"),
        P(None, "tp"),
        P("sp", "tp"),
        P("tp", None),
        P("tp", None),
        P("tp"),
        P("tp", None, None),
        P("tp", None, None),
        P("tp", None, None),
        P("tp", None, None),
        P("tp"),
        P("tp", "sp"),
        P("tp", "sp"),
    )
    return jax.shard_map(
        shards, mesh=mesh, in_specs=placed, out_specs=P(("fs", "sp", "tp"), None), check_vma=False
    )
```

profile of v0, /device:TPU:31, one launch (start us, length us, event | category | flops | bytes accessed | tf_op | source)
XLA Modules:
  0.0 690.0 jit_solution(16602157050290242901)
XLA Ops:
  15.0 1.8 compare_convert_fusion.3
  16.8 1.8 slice_compare_fusion.1
  25.1 37.8 %all-gather.4 = f32[32,1,4096]{2,1,0:T(1,128)S(1)} all-gather(f32[1,1,4096]{2,1,0:T(1,128)S(1)} %reshape.308), channel_id=1, replica_groups=mesh['sp'=32,'fs'=1,'tp'=1] {'sp'}, dimensions={0}, use_global_device_ids=true | all-gather | bytes 540672 | tf_op jit(solution)/shard_map/all_gather | solution.py:17
  63.3 40.8 %all-gather.3 = f32[32,1,4096]{2,1,0:T(1,128)S(1)} all-gather(f32[1,1,4096]{2,1,0:T(1,128)S(1)} %reshape.306), channel_id=1, replica_groups=mesh['sp'=32,'fs'=1,'tp'=1] {'sp'}, dimensions={0}, use_global_device_ids=true | all-gather | bytes 540672 | tf_op jit(solution)/shard_map/all_gather | solution.py:17
  105.1 39.2 %all-reduce.3 = (f32[32]{0:T(128)}, f32[32]{0:T(128)}) all-reduce(f32[32]{0:T(128)S(1)} %get-tuple-element.401, f32[32]{0:T(128)S(1)} %slice_dynamic-update-slice_fusion), channel_id=2, replica_groups=mesh['sp'=32,'fs'=1,'tp'=1] {'sp'}, use_global_device_ids=true, to_apply=%add.1 | all-reduce | flops 64 | bytes 512
  144.3 2.9 convolution_convert_fusion
  147.5 8.8 %fusion.35 = f32[64,64,16]{1,2,0:T(8,128)S(1)} fusion(bf16[128,64,16]{0,2,1:T(8,128)(2,1)S(1)} %bitcast.118, f32[64,64]{1,0:T(8,128)S(1)} %get-tuple-element.396, f32[128]{0:T(128)S(1)} %subtract_convert_fusion, f32[128]{0:T(128)S(1)} %get-tuple-element.406, f32[64,64]{1,0:T(8,128)S(1)} %get-tuple-element.395, f32[128]{0:T(128)S(1)} %fusion.89), kind=kOutput, calls=%fused_computation.60 | convolution fusion | flops 102760448 | bytes 558592 | tf_op jit(solution)/shard_map/tgp,tgh->gph/dot_general | solution.py:196
  156.2 11.2 %add_reduce_fusion = (f32[64,64]{1,0:T(8,128)S(1)}, f32[64,64]{1,0:T(8,128)S(1)}, f32[64,64,16]{1,2,0:T(8,128)S(1)}, f32[64,64,16]{1,2,0:T(8,128)S(1)}) fusion(f32[64,64,16]{1,2,0:T(8,128)S(1)} %fusion.35, f32[64,64,16]{1,2,0:T(8,128)} %param.34, f32[64,64]{1,0:T(8,128)S(1)} %get-tuple-element.393, f32[64,64,16]{1,2,0:T(8,128)} %param.33, ...), kind=kOutput, calls=%fused_computation.112 | convolution fusion | flops 103669760 | bytes 1672704 | tf_op jit(solution)/shard_map/tgp,tgh->gph/dot_general | solution.py:193
  167.5 40.3 %all-gather.5 = f32[32,1,4096]{2,1,0:T(1,128)S(1)} all-gather(f32[1,1,4096]{2,1,0:T(1,128)S(1)} %reshape.310), channel_id=1, replica_groups=mesh['sp'=32,'fs'=1,'tp'=1] {'sp'}, dimensions={0}, use_global_device_ids=true | all-gather | bytes 540672 | tf_op jit(solution)/shard_map/all_gather | solution.py:17
  208.1 41.1 %all-gather.2 = f32[32,1,4096]{2,1,0:T(1,128)S(1)} all-gather(f32[1,1,4096]{2,1,0:T(1,128)S(1)} %reshape.304), channel_id=1, replica_groups=mesh['sp'=32,'fs'=1,'tp'=1] {'sp'}, dimensions={0}, use_global_device_ids=true | all-gather | bytes 540672 | tf_op jit(solution)/shard_map/all_gather | solution.py:17
  250.3 147.9 %while.34 = (s32[]{:T(128)}, f32[4096]{0:T(1024)S(1)}, f32[4096]{0:T(1024)S(1)}, f32[1]{0:T(128)}, s32[]{:T(128)}, /*index=5*/f32[32,4096]{1,0:T(8,128)}, f32[32...) while((s32[]{:T(128)}, f32[4096]{0:T(1024)S(1)}, ...), condition=%wide.region_4.5_spmd, body=%wide.region_3.0_spmd.sunk | while | flops 40973 | bytes 262411 | solution.py:25
  400.5 262.8 %while.35 = (s32[]{:T(128)}, f32[4096]{0:T(1024)S(1)}, f32[4096]{0:T(1024)S(1)}, f32[8,16,1024]{2,1,0:T(8,128)}, f32[8,16]{1,0:T(8,128)}, /*index=5*/f32[8,16,10...) while((s32[]{:T(128)}, f32[4096]{0:T(1024)S(1)}, ...), condition=%wide.region_8.9_spmd.clone.clone, body=%wide.region_5.8_spmd.clone.clone.sunk | while | flops 65856800 | bytes 17222116 | solution.py:130
  405.1 18.7 %fusion.132 = (f32[16,4096]{1,0:T(8,128)S(1)}, f32[16,4096]{1,0:T(8,128)S(1)}) fusion(f32[4096]{0:T(1024)S(1)} %get-tuple-element.713, f32[16,16]{1,0:T(8,128)S(1)} %copy-done.22, f32[4096]{0:T(1024)S(1)} %get-tuple-element.711, f32[16,16]{1,0:T(8,128)S(1)} %copy-done.23, f32[16,4096]{1,0:T(8,128)S(1)} %mul.1494, f32[16,4096]{1,0:T(8,128)S(1)} %mul.1495, ...), kind=kLoop, calls=%fused_computation.27.clone.1 | loop fusion | flops 14548992 | bytes 1084416 | tf_op jit(solution)/shard_map/while/body/eval_jaxpr/reduce_sum | solution.py:113
  431.6 1.6 slice_add_fusion.3
  437.9 18.7 %fusion.132 = (f32[16,4096]{1,0:T(8,128)S(1)}, f32[16,4096]{1,0:T(8,128)S(1)}) fusion(f32[4096]{0:T(1024)S(1)} %get-tuple-element.713, f32[16,16]{1,0:T(8,128)S(1)} %copy-done.22, f32[4096]{0:T(1024)S(1)} %get-tuple-element.711, f32[16,16]{1,0:T(8,128)S(1)} %copy-done.23, f32[16,4096]{1,0:T(8,128)S(1)} %mul.1494, f32[16,4096]{1,0:T(8,128)S(1)} %mul.1495, ...), kind=kLoop, calls=%fused_computation.27.clone.1 | loop fusion | flops 14548992 | bytes 1084416 | tf_op jit(solution)/shard_map/while/body/eval_jaxpr/reduce_sum | solution.py:113
  464.4 1.6 slice_add_fusion.3
  470.7 18.7 %fusion.132 = (f32[16,4096]{1,0:T(8,128)S(1)}, f32[16,4096]{1,0:T(8,128)S(1)}) fusion(f32[4096]{0:T(1024)S(1)} %get-tuple-element.713, f32[16,16]{1,0:T(8,128)S(1)} %copy-done.22, f32[4096]{0:T(1024)S(1)} %get-tuple-element.711, f32[16,16]{1,0:T(8,128)S(1)} %copy-done.23, f32[16,4096]{1,0:T(8,128)S(1)} %mul.1494, f32[16,4096]{1,0:T(8,128)S(1)} %mul.1495, ...), kind=kLoop, calls=%fused_computation.27.clone.1 | loop fusion | flops 14548992 | bytes 1084416 | tf_op jit(solution)/shard_map/while/body/eval_jaxpr/reduce_sum | solution.py:113
  497.3 1.6 slice_add_fusion.3
  503.5 18.7 %fusion.132 = (f32[16,4096]{1,0:T(8,128)S(1)}, f32[16,4096]{1,0:T(8,128)S(1)}) fusion(f32[4096]{0:T(1024)S(1)} %get-tuple-element.713, f32[16,16]{1,0:T(8,128)S(1)} %copy-done.22, f32[4096]{0:T(1024)S(1)} %get-tuple-element.711, f32[16,16]{1,0:T(8,128)S(1)} %copy-done.23, f32[16,4096]{1,0:T(8,128)S(1)} %mul.1494, f32[16,4096]{1,0:T(8,128)S(1)} %mul.1495, ...), kind=kLoop, calls=%fused_computation.27.clone.1 | loop fusion | flops 14548992 | bytes 1084416 | tf_op jit(solution)/shard_map/while/body/eval_jaxpr/reduce_sum | solution.py:113
  530.1 1.6 slice_add_fusion.3
  536.3 18.7 %fusion.132 = (f32[16,4096]{1,0:T(8,128)S(1)}, f32[16,4096]{1,0:T(8,128)S(1)}) fusion(f32[4096]{0:T(1024)S(1)} %get-tuple-element.713, f32[16,16]{1,0:T(8,128)S(1)} %copy-done.22, f32[4096]{0:T(1024)S(1)} %get-tuple-element.711, f32[16,16]{1,0:T(8,128)S(1)} %copy-done.23, f32[16,4096]{1,0:T(8,128)S(1)} %mul.1494, f32[16,4096]{1,0:T(8,128)S(1)} %mul.1495, ...), kind=kLoop, calls=%fused_computation.27.clone.1 | loop fusion | flops 14548992 | bytes 1084416 | tf_op jit(solution)/shard_map/while/body/eval_jaxpr/reduce_sum | solution.py:113
  562.9 1.6 slice_add_fusion.3
  569.2 18.7 %fusion.132 = (f32[16,4096]{1,0:T(8,128)S(1)}, f32[16,4096]{1,0:T(8,128)S(1)}) fusion(f32[4096]{0:T(1024)S(1)} %get-tuple-element.713, f32[16,16]{1,0:T(8,128)S(1)} %copy-done.22, f32[4096]{0:T(1024)S(1)} %get-tuple-element.711, f32[16,16]{1,0:T(8,128)S(1)} %copy-done.23, f32[16,4096]{1,0:T(8,128)S(1)} %mul.1494, f32[16,4096]{1,0:T(8,128)S(1)} %mul.1495, ...), kind=kLoop, calls=%fused_computation.27.clone.1 | loop fusion | flops 14548992 | bytes 1084416 | tf_op jit(solution)/shard_map/while/body/eval_jaxpr/reduce_sum | solution.py:113
  595.7 1.6 slice_add_fusion.3
  602.0 18.7 %fusion.132 = (f32[16,4096]{1,0:T(8,128)S(1)}, f32[16,4096]{1,0:T(8,128)S(1)}) fusion(f32[4096]{0:T(1024)S(1)} %get-tuple-element.713, f32[16,16]{1,0:T(8,128)S(1)} %copy-done.22, f32[4096]{0:T(1024)S(1)} %get-tuple-element.711, f32[16,16]{1,0:T(8,128)S(1)} %copy-done.23, f32[16,4096]{1,0:T(8,128)S(1)} %mul.1494, f32[16,4096]{1,0:T(8,128)S(1)} %mul.1495, ...), kind=kLoop, calls=%fused_computation.27.clone.1 | loop fusion | flops 14548992 | bytes 1084416 | tf_op jit(solution)/shard_map/while/body/eval_jaxpr/reduce_sum | solution.py:113
  628.5 1.6 slice_add_fusion.3
  634.8 18.7 %fusion.132 = (f32[16,4096]{1,0:T(8,128)S(1)}, f32[16,4096]{1,0:T(8,128)S(1)}) fusion(f32[4096]{0:T(1024)S(1)} %get-tuple-element.713, f32[16,16]{1,0:T(8,128)S(1)} %copy-done.22, f32[4096]{0:T(1024)S(1)} %get-tuple-element.711, f32[16,16]{1,0:T(8,128)S(1)} %copy-done.23, f32[16,4096]{1,0:T(8,128)S(1)} %mul.1494, f32[16,4096]{1,0:T(8,128)S(1)} %mul.1495, ...), kind=kLoop, calls=%fused_computation.27.clone.1 | loop fusion | flops 14548992 | bytes 1084416 | tf_op jit(solution)/shard_map/while/body/eval_jaxpr/reduce_sum | solution.py:113
  661.3 1.6 slice_add_fusion.3
  663.4 3.2 fusion.40
  666.7 2.9 fusion.39
  672.8 5.8 fusion.57
  678.7 4.5 fusion.30
  (676 shorter events, 189.3 us)
Async XLA Ops:
  6.5 137.8 %copy-start.6 = (bf16[128,2048]{1,0:T(8,128)(2,1)S(1)}, bf16[128,2048]{1,0:T(8,128)(2,1)}, u32[]{:S(2)}) copy-start(bf16[128,2048]{1,0:T(8,128)(2,1)} %param.22) | copy-start | bytes 1572868
  6.5 98.0 %copy-start.17 = (bf16[3,1024]{1,0:T(4,128)(2,1)S(1)}, bf16[3,1024]{1,0:T(4,128)(2,1)}, u32[]{:S(2)}) copy-start(bf16[3,1024]{1,0:T(4,128)(2,1)} %param.28) | copy-start | bytes 18436
  6.5 137.8 %all-gather.19.cloned.1.call-start = ((), (), s32[]{:S(2)}) async-start(), calls=%async_computation.3 | async-start | bytes 4325376 | tf_op jit(solution)/shard_map/all_gather | solution.py:177
  7.3 656.1 %all-gather.15.cloned.1.call-start = ((), (), s32[]{:S(2)}) async-start(), calls=%async_computation.1 | async-start | bytes 4325376 | tf_op jit(solution)/shard_map/all_gather | solution.py:175
  8.0 658.6 %all-gather.17.cloned.1.call-start = ((), (), s32[]{:S(2)}) async-start(), calls=%async_computation.2 | async-start | bytes 4325376 | tf_op jit(solution)/shard_map/all_gather | solution.py:176
  8.7 662.6 %all-gather.13.cloned.1.call-start = ((), (), s32[]{:S(2)}) async-start(), calls=%async_computation | async-start | bytes 4325376 | tf_op jit(solution)/shard_map/all_gather | solution.py:174
  9.3 662.0 %all-gather.21.cloned.1.call-start = ((), (), s32[]{:S(2)}) async-start(), calls=%async_computation.4 | async-start | bytes 4325376 | tf_op jit(solution)/shard_map/all_gather | solution.py:265
  9.9 668.7 %all-gather.23.cloned.1.call-start = ((), (), s32[]{:S(2)}) async-start(), calls=%async_computation.5 | async-start | bytes 4325376 | tf_op jit(solution)/shard_map/all_gather | solution.py:266
  21.2 126.1 %copy-start.14 = (f32[2048]{0:T(1024)}, f32[2048]{0:T(1024)S(1)}, u32[]{:S(2)}) copy-start(f32[2048]{0:T(1024)S(1)} %convert_element_type.100) | copy-start | bytes 24580
  22.4 124.9 %copy-start.26 = (f32[128]{0:T(128)}, f32[128]{0:T(128)S(1)}, u32[]{:S(2)}) copy-start(f32[128]{0:T(128)S(1)} %add_rsqrt_fusion) | copy-start | bytes 1540
  147.3 252.4 %copy-start.9 = (bf16[128,1024]{1,0:T(8,128)(2,1)}, bf16[128,1024]{1,0:T(8,128)(2,1)S(1)}, u32[]{:S(2)}) copy-start(bf16[128,1024]{1,0:T(8,128)(2,1)S(1)} %convolution_convert_fusion) | copy-start | bytes 786436
  167.4 233.1 %copy-start = (f32[64,16,64]{2,1,0:T(8,128)S(1)}, f32[64,16,64]{2,1,0:T(8,128)}, u32[]{:S(2)}) copy-start(f32[64,16,64]{2,1,0:T(8,128)} %param.35) | copy-start | bytes 786436
  400.5 23.3 %copy-start.1 = (f32[64,64,16]{1,2,0:T(8,128)}, f32[64,64,16]{1,2,0:T(8,128)S(1)}, u32[]{:S(2)}) copy-start(f32[64,64,16]{1,2,0:T(8,128)S(1)} %get-tuple-element.706) | copy-start | bytes 786436 | tf_op jit(solution)/shard_map/while
  400.5 24.3 %copy-start.11 = (f32[4096]{0:T(1024)}, f32[4096]{0:T(1024)S(1)}, u32[]{:S(2)}) copy-start(f32[4096]{0:T(1024)S(1)} %get-tuple-element.713) | copy-start | bytes 49156 | tf_op jit(solution)/shard_map/while
  404.9 19.9 %copy-start.18 = (f32[16]{0:T(128)S(1)}, f32[16]{0:T(128)}, u32[]{:S(2)}) copy-start(f32[16]{0:T(128)} %get-tuple-element.716) | copy-start | bytes 196 | tf_op jit(solution)/shard_map/while
  433.3 23.3 %copy-start.1 = (f32[64,64,16]{1,2,0:T(8,128)}, f32[64,64,16]{1,2,0:T(8,128)S(1)}, u32[]{:S(2)}) copy-start(f32[64,64,16]{1,2,0:T(8,128)S(1)} %get-tuple-element.706) | copy-start | bytes 786436 | tf_op jit(solution)/shard_map/while
  433.3 24.3 %copy-start.11 = (f32[4096]{0:T(1024)}, f32[4096]{0:T(1024)S(1)}, u32[]{:S(2)}) copy-start(f32[4096]{0:T(1024)S(1)} %get-tuple-element.713) | copy-start | bytes 49156 | tf_op jit(solution)/shard_map/while
  437.7 19.9 %copy-start.18 = (f32[16]{0:T(128)S(1)}, f32[16]{0:T(128)}, u32[]{:S(2)}) copy-start(f32[16]{0:T(128)} %get-tuple-element.716) | copy-start | bytes 196 | tf_op jit(solution)/shard_map/while
  466.1 23.3 %copy-start.1 = (f32[64,64,16]{1,2,0:T(8,128)}, f32[64,64,16]{1,2,0:T(8,128)S(1)}, u32[]{:S(2)}) copy-start(f32[64,64,16]{1,2,0:T(8,128)S(1)} %get-tuple-element.706) | copy-start | bytes 786436 | tf_op jit(solution)/shard_map/while
  466.1 24.3 %copy-start.11 = (f32[4096]{0:T(1024)}, f32[4096]{0:T(1024)S(1)}, u32[]{:S(2)}) copy-start(f32[4096]{0:T(1024)S(1)} %get-tuple-element.713) | copy-start | bytes 49156 | tf_op jit(solution)/shard_map/while
  470.5 19.9 %copy-start.18 = (f32[16]{0:T(128)S(1)}, f32[16]{0:T(128)}, u32[]{:S(2)}) copy-start(f32[16]{0:T(128)} %get-tuple-element.716) | copy-start | bytes 196 | tf_op jit(solution)/shard_map/while
  498.9 23.3 %copy-start.1 = (f32[64,64,16]{1,2,0:T(8,128)}, f32[64,64,16]{1,2,0:T(8,128)S(1)}, u32[]{:S(2)}) copy-start(f32[64,64,16]{1,2,0:T(8,128)S(1)} %get-tuple-element.706) | copy-start | bytes 786436 | tf_op jit(solution)/shard_map/while
  499.0 24.3 %copy-start.11 = (f32[4096]{0:T(1024)}, f32[4096]{0:T(1024)S(1)}, u32[]{:S(2)}) copy-start(f32[4096]{0:T(1024)S(1)} %get-tuple-element.713) | copy-start | bytes 49156 | tf_op jit(solution)/shard_map/while
  531.8 23.3 %copy-start.1 = (f32[64,64,16]{1,2,0:T(8,128)}, f32[64,64,16]{1,2,0:T(8,128)S(1)}, u32[]{:S(2)}) copy-start(f32[64,64,16]{1,2,0:T(8,128)S(1)} %get-tuple-element.706) | copy-start | bytes 786436 | tf_op jit(solution)/shard_map/while
  531.8 24.3 %copy-start.11 = (f32[4096]{0:T(1024)}, f32[4096]{0:T(1024)S(1)}, u32[]{:S(2)}) copy-start(f32[4096]{0:T(1024)S(1)} %get-tuple-element.713) | copy-start | bytes 49156 | tf_op jit(solution)/shard_map/while
  564.6 23.3 %copy-start.1 = (f32[64,64,16]{1,2,0:T(8,128)}, f32[64,64,16]{1,2,0:T(8,128)S(1)}, u32[]{:S(2)}) copy-start(f32[64,64,16]{1,2,0:T(8,128)S(1)} %get-tuple-element.706) | copy-start | bytes 786436 | tf_op jit(solution)/shard_map/while
  564.6 24.3 %copy-start.11 = (f32[4096]{0:T(1024)}, f32[4096]{0:T(1024)S(1)}, u32[]{:S(2)}) copy-start(f32[4096]{0:T(1024)S(1)} %get-tuple-element.713) | copy-start | bytes 49156 | tf_op jit(solution)/shard_map/while
  597.4 23.3 %copy-start.1 = (f32[64,64,16]{1,2,0:T(8,128)}, f32[64,64,16]{1,2,0:T(8,128)S(1)}, u32[]{:S(2)}) copy-start(f32[64,64,16]{1,2,0:T(8,128)S(1)} %get-tuple-element.706) | copy-start | bytes 786436 | tf_op jit(solution)/shard_map/while
  597.4 24.3 %copy-start.11 = (f32[4096]{0:T(1024)}, f32[4096]{0:T(1024)S(1)}, u32[]{:S(2)}) copy-start(f32[4096]{0:T(1024)S(1)} %get-tuple-element.713) | copy-start | bytes 49156 | tf_op jit(solution)/shard_map/while
  630.2 23.3 %copy-start.1 = (f32[64,64,16]{1,2,0:T(8,128)}, f32[64,64,16]{1,2,0:T(8,128)S(1)}, u32[]{:S(2)}) copy-start(f32[64,64,16]{1,2,0:T(8,128)S(1)} %get-tuple-element.706) | copy-start | bytes 786436 | tf_op jit(solution)/shard_map/while
  630.2 24.3 %copy-start.11 = (f32[4096]{0:T(1024)}, f32[4096]{0:T(1024)S(1)}, u32[]{:S(2)}) copy-start(f32[4096]{0:T(1024)S(1)} %get-tuple-element.713) | copy-start | bytes 49156 | tf_op jit(solution)/shard_map/while
  669.7 3.0 collective-permute-start
  (114 other events, 684.2 us)
Sparse Core Ops, SparseCore 0:
  10.2 62.3 all-gather.18
  75.5 60.5 all-gather.14
  138.9 62.1 all-gather.16
  203.8 60.8 all-gather.12
  267.4 60.5 all-gather.20
  330.7 60.4 all-gather.22
where the time goes:
time: 694 us; the launch traced here: 690 us
  blocking collectives  199 us (29%)
  other arithmetic  196 us (28%)
  local copies, waits for them, and re-layouts  118 us (17%)
  loops' own time  80.8 us (12%)
  matrix products  73.7 us (11%)
  between operations  15.7 us (2%)
    all_gather x4, blocking collectives, prefix(): gathered = jax.tree.map(lambda a: lax.all_gather(a, axis), part)  160 us
    reduce_sum x8, other arithmetic, one_block(): jnp.sum(weigh_real * push_imag[None, :, :] + weigh_imag * push_real[None,...  149 us
    another operation x1, loops' own time, prefix(): return lax.fori_loop(0, place, one, state)  78 us
    dynamic_slice x93, local copies, waits for them, and re-layouts, one(): lax.dynamic_index_in_dim(a, turn, 0, False)  69.4 us
    unnamed x1, blocking collectives  39.2 us
    add x16, other arithmetic, one_block(): jnp.sum(weigh_real * push_imag[None, :, :] + weigh_imag * push_real[None,...  20.5 us
  transfers between devices with their start and end apart: 7, of which 1 were waited for; matrix products, arithmetic and copies ran while one was open for 55% of the time, Pallas kernels for 0%

commit v1 on v0

v1 whole, which is shorter than its diff:
```python
import functools
import math

import jax
import jax.numpy as jnp
from jax import lax
from jax.experimental import pallas as pl
from jax.experimental.pallas import tpu as pltpu
from jax.sharding import PartitionSpec as P

D = 2048
TAPS = 3
TILE = 8
REACHES = (1, 2, 4)


EPS = 1e-06


def from_behind(block, axis, distance):
    devices = range(lax.axis_size(axis))
    route = [(i - distance, i) for i in devices if i - distance in devices]
    return lax.ppermute(block, axis, route)


def ssm_constants(decay_rate, frequency, step_log, input_real, input_imag):
    step_size = jnp.exp(step_log)[:, None]
    damping = decay_rate * step_size
    turning = frequency * step_size
    fading = jnp.exp(-damping)
    coef_imag = fading * jnp.sin(turning)
    half_sine = jnp.sin(turning / 2.0)
    less_real = jnp.expm1(-damping) * jnp.cos(turning) - 2.0 * half_sine * half_sine
    denominator = decay_rate * decay_rate + frequency * frequency
    ratio_real = (-less_real * decay_rate + coef_imag * frequency) / denominator
    ratio_imag = (-coef_imag * decay_rate - less_real * frequency) / denominator
    bbar_real = ratio_real[..., None] * input_real - ratio_imag[..., None] * input_imag
    bbar_imag = ratio_real[..., None] * input_imag + ratio_imag[..., None] * input_real
    return (bbar_real, bbar_imag, damping.reshape(-1), turning.reshape(-1))


def spread(rows, group_size):
    lanes, state_size = rows.shape
    reps = lanes // group_size
    wide = jnp.concatenate([rows] * reps, axis=1)
    row = lax.broadcasted_iota(jnp.int32, wide.shape, 0) // group_size
    col = lax.broadcasted_iota(jnp.int32, wide.shape, 1) // state_size
    return jnp.where(row == col, wide, 0.0).astype(jnp.bfloat16)


def scan_rows(u, b_re, b_im, pow_re, pow_im, masks, start_re, start_im, keep):
    push_re = jnp.dot(u, b_re, preferred_element_type=jnp.float32)
    push_im = jnp.dot(u, b_im, preferred_element_type=jnp.float32)
    carry_re, carry_im = start_re, start_im
    for begin in range(0, u.shape[0], TILE):
        x_re = push_re[begin : begin + TILE]
        x_im = push_im[begin : begin + TILE]
        for slot, reach in enumerate(REACHES):
            m = masks[begin : begin + TILE, slot : slot + 1]
            p_re = pow_re[reach - 1 : reach] * m
            p_im = pow_im[reach - 1 : reach] * m
            s_re = pltpu.roll(x_re, reach, 0)
            s_im = pltpu.roll(x_im, reach, 0)
            x_re, x_im = x_re + (p_re * s_re - p_im * s_im), x_im + (p_re * s_im + p_im * s_re)
        m = masks[begin : begin + TILE, len(REACHES) : len(REACHES) + 1]
        p_re, p_im = pow_re * m, pow_im * m
        x_re, x_im = (
            x_re + (p_re * carry_re - p_im * carry_im),
            x_im + (p_re * carry_im + p_im * carry_re),
        )
        carry_re, carry_im = x_re[TILE - 1 :], x_im[TILE - 1 :]
        keep(begin, x_re, x_im)
    return carry_re, carry_im


def ends_body(group_size, u_ref, bre_ref, bim_ref, pre_ref, pim_ref, mask_ref, ere_ref, eim_ref):
    zero = jnp.zeros((1, pre_ref.shape[-1]), jnp.float32)
    end_re, end_im = scan_rows(
        u_ref[...],
        spread(bre_ref[...], group_size),
        spread(bim_ref[...], group_size),
        pre_ref[0],
        pim_ref[0],
        mask_ref[...],
        zero,
        zero,
        lambda begin, x_re, x_im: None,
    )
    ere_ref[0] = end_re
    eim_ref[0] = end_im


def join_body(keep_ref, take_ref, end_ref, dec_ref, sre_ref, sim_ref):
    dec_re, dec_im = dec_ref[0], dec_ref[1]
    s_re = jnp.zeros(dec_re.shape, jnp.float32)
    s_im = s_re
    for turn in range(end_ref.shape[0]):
        keep, take = keep_ref[turn], take_ref[turn]
        n_re = dec_re * s_re - dec_im * s_im + end_ref[turn, 0]
        n_im = dec_re * s_im + dec_im * s_re + end_ref[turn, 1]
        s_re, s_im = keep * s_re + take * n_re, keep * s_im + take * n_im
    sre_ref[...] = s_re
    sim_ref[...] = s_im


def mix_body(
    group_size, u_ref, bre_ref, bim_ref, cre_ref, cim_ref, pre_ref, pim_ref, mask_ref,
    sre_ref, sim_ref, skip_ref, out_ref, hre_ref, him_ref,
):
    def keep(begin, x_re, x_im):
        hre_ref[begin : begin + TILE, :] = x_re
        him_ref[begin : begin + TILE, :] = x_im

    u = u_ref[...]
    scan_rows(
        u,
        spread(bre_ref[...], group_size),
        spread(bim_ref[...], group_size),
        pre_ref[0],
        pim_ref[0],
        mask_ref[...],
        sre_ref[0],
        sim_ref[0],
        keep,
    )
    along = (((1,), (1,)), ((), ()))
    y = lax.dot_general(
        hre_ref[...].astype(jnp.bfloat16),
        spread(cre_ref[...], group_size),
        along,
        preferred_element_type=jnp.float32,
    ) - lax.dot_general(
        him_ref[...].astype(jnp.bfloat16),
        spread(cim_ref[...], group_size),
        along,
        preferred_element_type=jnp.float32,
    )
    y = y + skip_ref[...] * u.astype(jnp.float32)
    out_ref[...] = jax.nn.gelu(y, approximate=True).astype(jnp.bfloat16)


def block_specs(rows, lanes, state_size, span):
    return dict(
        u=pl.BlockSpec((rows, lanes), lambda j: (0, j)),
        mat=pl.BlockSpec((lanes, state_size), lambda j: (j, 0)),
        pow=pl.BlockSpec((1, TILE, span), lambda j: (j, 0, 0)),
        mask=pl.BlockSpec((rows, len(REACHES) + 1), lambda j: (0, 0)),
        state=pl.BlockSpec((1, 1, span), lambda j: (j, 0, 0)),
        skip=pl.BlockSpec((1, lanes), lambda j: (0, j)),
    )


def shards(
    tokens,
    documents,
    norm_gain,
    out_gate_weight,
    in_gate_weight,
    value_weight,
    conv_taps,
    state_in_weight,
    decay_rate,
    frequency,
    step_log,
    input_real,
    input_imag,
    readout_real,
    readout_imag,
    skip_gain,
    conv_out_weight,
    state_out_weight,
):
    row_count = tokens.shape[0]
    groups, state_size = decay_rate.shape
    group_size = input_real.shape[2]
    values = tokens.astype(jnp.float32)
    totals = lax.psum(jnp.sum(values * values, axis=1), "tp")
    scaled = values * lax.rsqrt(totals / D + EPS)[:, None] * norm_gain.astype(jnp.float32)[None, :]
    normed = lax.all_gather(scaled.astype(jnp.bfloat16), "tp", axis=1, tiled=True)
    bbar_real, bbar_imag, damping, turning = ssm_constants(
        decay_rate, frequency, step_log, input_real, input_imag
    )
    doc_float = documents.astype(jnp.float32)
    pieces = (
        lax.all_gather(out_gate_weight, "sp", axis=0, tiled=True),
        lax.all_gather(in_gate_weight, "sp", axis=0, tiled=True),
        lax.all_gather(value_weight, "sp", axis=0, tiled=True),
        lax.all_gather(state_in_weight, "sp", axis=0, tiled=True),
    )
    gate_sum, inner_sum, value_sum, driven_sum = tuple(
        (jnp.dot(normed, piece, preferred_element_type=jnp.float32) for piece in pieces)
    )
    driven = driven_sum.astype(jnp.bfloat16)
    place = lax.axis_index("sp")
    devices = lax.axis_size("sp")
    lasts = lax.all_gather(doc_float[-1], "sp")
    in_last = jnp.where(place > 0, lasts[jnp.maximum(place - 1, 0)], -1.0)
    lanes = math.gcd(groups * group_size, 128)
    blocks = groups * group_size // lanes
    span = lanes // group_size * state_size
    order = jnp.arange(row_count)
    columns = [
        (order % TILE >= reach) & (documents == jnp.roll(documents, reach)) for reach in REACHES
    ]
    before = jnp.concatenate([in_last[None], doc_float[TILE - 1 : -1 : TILE]])
    columns.append(doc_float == jnp.repeat(before, TILE))
    masks = jnp.stack(columns, axis=1).astype(jnp.float32)
    counts = jnp.arange(1, TILE + 1, dtype=jnp.float32)[None, :, None]
    damp = damping.reshape(blocks, 1, span)
    turn = turning.reshape(blocks, 1, span)
    fade = jnp.exp(-counts * damp)
    pow_re, pow_im = fade * jnp.cos(counts * turn), fade * jnp.sin(counts * turn)
    damp, turn = damp[:, 0], turn[:, 0]
    whole = jnp.exp(-row_count * damp)
    decay = jnp.stack([whole * jnp.cos(row_count * turn), whole * jnp.sin(row_count * turn)])
    b_re = jnp.swapaxes(bbar_real, 1, 2).reshape(groups * group_size, state_size)
    b_im = jnp.swapaxes(bbar_imag, 1, 2).reshape(groups * group_size, state_size)
    c_re = readout_real.reshape(groups * group_size, state_size)
    c_im = readout_imag.reshape(groups * group_size, state_size)
    spec = block_specs(row_count, lanes, state_size, span)
    state_shape = jax.ShapeDtypeStruct((blocks, 1, span), jnp.float32)
    ends = pl.pallas_call(
        functools.partial(ends_body, group_size),
        grid=(blocks,),
        in_specs=[spec[k] for k in ("u", "mat", "mat", "pow", "pow", "mask")],
        out_specs=[spec["state"]] * 2,
        out_shape=[state_shape] * 2,
        name="ends",
    )(driven, b_re, b_im, pow_re, pow_im, masks)
    ends = lax.all_gather(jnp.stack([e.reshape(blocks, span) for e in ends]), "sp")
    source = jnp.arange(devices)
    take = ((source < place) & (lasts == in_last)).astype(jnp.float32)
    later = (source >= place).astype(jnp.float32)
    scalar = pl.BlockSpec(memory_space=pltpu.SMEM)
    vector = pl.BlockSpec(memory_space=pltpu.VMEM)
    start_re, start_im = pl.pallas_call(
        join_body,
        in_specs=[scalar, scalar, vector, vector],
        out_specs=[vector] * 2,
        out_shape=[jax.ShapeDtypeStruct((blocks, span), jnp.float32)] * 2,
        name="join",
    )(later, take, ends, decay)
    ssm_out = pl.pallas_call(
        functools.partial(mix_body, group_size),
        grid=(blocks,),
        in_specs=[
            spec[k]
            for k in (
                "u", "mat", "mat", "mat", "mat", "pow", "pow", "mask", "state", "state", "skip",
            )
        ],
        out_specs=spec["u"],
        out_shape=jax.ShapeDtypeStruct(driven.shape, jnp.bfloat16),
        scratch_shapes=[pltpu.VMEM((row_count, span), jnp.float32)] * 2,
        name="mix",
    )(
        driven, b_re, b_im, c_re, c_im, pow_re, pow_im, masks,
        start_re[:, None], start_im[:, None], skip_gain[None],
    )
    out_gate = gate_sum.astype(jnp.bfloat16).astype(jnp.float32)
    in_gate = inner_sum.astype(jnp.bfloat16).astype(jnp.float32)
    value = value_sum.astype(jnp.bfloat16).astype(jnp.float32)
    product = (in_gate * value).astype(jnp.bfloat16)
    margin = TAPS - 1
    tail_same = documents[row_count - margin :] == documents[-1]
    tail_rows = jnp.where(
        tail_same[:, None], product[row_count - margin :], jnp.zeros_like(product[:margin])
    )
    rim_rows = from_behind(tail_rows, "sp", 1)
    padded = jnp.concatenate([rim_rows, product], axis=0)
    padded_docs = jnp.concatenate([jnp.broadcast_to(in_last[None], (margin,)), doc_float], axis=0)
    total = jnp.zeros(product.shape, jnp.float32)
    for index in range(TAPS):
        same_doc = (padded_docs[index : index + row_count] == doc_float).astype(jnp.float32)
        total = (
            total
            + conv_taps[index].astype(jnp.float32)[None, :]
            * padded[index : index + row_count].astype(jnp.float32)
            * same_doc[:, None]
        )
    conv_out = (out_gate * total).astype(jnp.bfloat16)
    conv_columns, state_columns = (
        lax.all_gather(conv_out_weight, "sp", axis=1, tiled=True),
        lax.all_gather(state_out_weight, "sp", axis=1, tiled=True),
    )
    return lax.psum_scatter(
        (
            jnp.dot(conv_out, conv_columns, preferred_element_type=jnp.float32)
            + jnp.dot(ssm_out, state_columns, preferred_element_type=jnp.float32)
        ).astype(jnp.bfloat16),
        "tp",
        scatter_dimension=0,
        tiled=True,
    )


def solution(mesh):
    placed = (
        P(("fs", "sp"), "tp"),
        P(("fs", "sp")),
        P("tp"),
        P("sp", "tp"),
        P("sp", "tp"),
        P("sp", "tp"),
        P(None, "tp"),
        P("sp", "tp"),
        P("tp", None),
        P("tp", None),
        P("tp"),
        P("tp", None, None),
        P("tp", None, None),
        P("tp", None, None),
        P("tp", None, None),
        P("tp"),
        P("tp", "sp"),
        P("tp", "sp"),
    )
    return jax.shard_map(
        shards, mesh=mesh, in_specs=placed, out_specs=P(("fs", "sp", "tp"), None), check_vma=False
    )
```

time: 694 us -> 460 us (0.66)
  waiting for transfers between devices: 5.14 us -> 341 us
  other arithmetic: 196 us -> 12.9 us
  blocking collectives: 199 us -> 38.3 us
  local copies, waits for them, and re-layouts: 118 us -> 8.07 us
  loops' own time: 80.8 us -> 0 us
  matrix products: 73.7 us -> 19.9 us
  Pallas kernels: 0 us -> 18.9 us
    all_gather x4 -> x0, blocking collectives: 160 us -> none  [prefix(): gathered = jax.tree.map(lambda a: lax.all_gather(a, axis), part)]
    reduce_sum x8 -> x0, other arithmetic: 149 us -> none  [one_block(): jnp.sum(weigh_real * push_imag[None, :, :] + weigh_imag * push_real[None,...]
    dynamic_slice x109 -> x1, local copies, waits for them, and re-layouts: 82.4 us -> 0.58 us  [shards(): in_last = jnp.where(place > 0, lasts[jnp.maximum(place - 1, 0)], -1.0)]
    another operation x2 -> x0, loops' own time: 80.8 us -> none  [the longest x1 78 us: prefix(): return lax.fori_loop(0, place, one, state)]
    all_gather x1, waiting for transfers between devices: 0.01 us -> 63.2 us  [shards(): lax.all_gather(out_gate_weight, 'sp', axis=0, tiled=True)]
    all_gather x1, waiting for transfers between devices: 0.02 us -> 60.5 us  [shards(): lax.all_gather(value_weight, 'sp', axis=0, tiled=True)]
    all_gather x1, waiting for transfers between devices: 0.01 us -> 58.4 us  [shards(): lax.all_gather(conv_out_weight, 'sp', axis=1, tiled=True)]
    dot_general x34 -> x0, matrix products: 54.3 us -> none  [the longest x1 11.2 us: shards(): jnp.einsum('tgp,tgh->gph', weigh_real, split_rows, precision=lax.Precisio...]
  transfers between devices with their start and end apart: 7 -> 8, of which waited for: 1 -> 7; matrix products, arithmetic and copies ran while one was open for 55% -> 8% of each run, Pallas kernels for 0% -> 4%
where the time goes in v1:
time: 460 us; the launch traced here: 454 us
  waiting for transfers between devices  341 us (74%)
  blocking collectives  38.3 us (8%)
  matrix products  19.9 us (4%)
  Pallas kernels  18.9 us (4%)
  between operations  14.2 us (3%)
  other arithmetic  12.9 us (3%)
  local copies, waits for them, and re-layouts  8.07 us (2%)
    all_gather x1, waiting for transfers between devices, shards(): lax.all_gather(out_gate_weight, 'sp', axis=0, tiled=True)  63.2 us
    all_gather x1, waiting for transfers between devices, shards(): lax.all_gather(value_weight, 'sp', axis=0, tiled=True)  60.5 us
    all_gather x1, waiting for transfers between devices, shards(): lax.all_gather(conv_out_weight, 'sp', axis=1, tiled=True)  58.4 us
    all_gather x1, waiting for transfers between devices, shards(): lax.all_gather(state_out_weight, 'sp', axis=1, tiled=True)  49.6 us
    all_gather x1, waiting for transfers between devices, shards(): lax.all_gather(jnp.stack([e.reshape(blocks, span) for e in ends]), 'sp')  49.4 us
    all_gather x1, waiting for transfers between devices, shards(): lax.all_gather(in_gate_weight, 'sp', axis=0, tiled=True)  47.6 us
    unnamed x1, blocking collectives  38.3 us
    dot_general x3, matrix products, shards(): jnp.dot(normed, piece, preferred_element_type=jnp.float32)  9.54 us
  transfers between devices with their start and end apart: 8, of which 7 were waited for; matrix products, arithmetic and copies ran while one was open for 8% of the time, Pallas kernels for 4%

profile of v1, /device:TPU:31, one launch (start us, length us, event | category | flops | bytes accessed | tf_op | source)
XLA Modules:
  0.0 454.5 jit_solution(7077072180769225733)
XLA Ops:
  6.5 0.7 all-gather.17.cloned.1.call-update
  7.3 0.7 all-gather.11.cloned.1.call-update
  10.8 38.3 %all-reduce.1 = f32[32]{0:T(128)S(1)} all-reduce(f32[32]{0:T(128)S(1)} %slice_dynamic-update-slice_fusion), channel_id=1, replica_groups=mesh['sp'=32,'fs'=1,'tp'=1] {'sp'}, use_global_device_ids=true, to_apply=%add.1 | all-reduce | flops 32 | bytes 256
  49.2 1.2 slice.58
  50.5 0.7 slice.57
  51.2 0.7 slice.69
  53.4 1.5 and_bitcast_fusion.2
  56.4 1.2 cosine_multiply_fusion
  57.8 0.7 convert_element_type.76
  58.5 1.2 fusion.8
  59.7 1.3 fusion.33
  61.0 2.3 multiply_add_fusion
  63.3 7.9 %all-gather.17.cloned.1.call-done = bf16[2048,1024]{1,0:T(8,128)(2,1)} async-done(((bf16[64,1024]{1,0:T(8,128)(2,1)}), bf16[2048,1024]{1,0:T(8,128)(2,1)}) %all-gather.17.cloned.1.call-update) | async-done | bytes 4194320 | tf_op jit(solution)/shard_map/all_gather | solution.py:188
  71.2 3.6 convolution_convert_fusion.u_ref
  74.8 7.8 %ends.1 = (f32[8,1,512]{2,1,0:T(1,128)}, f32[8,1,512]{2,1,0:T(1,128)}) custom-call(bf16[128,1024]{1,0:T(8,128)(2,1)} %convolution_convert_fusion.u_ref, f32[1024,64]{1,0:T(8,128)} %bitcast.38, f32[1024,64]{1,0:T(8,128)} %bitcast.36, f32[8,8,512]{2,1,0:T(8,128)} %get-tuple-element.20.pre_ref, f32[8,8,512]{2,1,0:T(8,128)} %get-tuple-element.19.pim_ref, ...), custom_call_target="tpu_custom_call" | custom-call | tf_op jit(solution)/shard_map/ends/pallas_call | solution.py:222
  82.6 0.8 pad_maximum_fusion.2
  84.1 0.7 all-gather.19.cloned.1.call-update
  86.8 47.6 %all-gather.11.cloned.1.call-done = bf16[2048,1024]{1,0:T(8,128)(2,1)} async-done(((bf16[64,1024]{1,0:T(8,128)(2,1)}), bf16[2048,1024]{1,0:T(8,128)(2,1)}) %all-gather.11.cloned.1.call-update) | async-done | bytes 4194320 | tf_op jit(solution)/shard_map/all_gather | solution.py:186
  134.4 2.9 fusion.4
  137.4 60.5 %all-gather.13.cloned.1.call-done = bf16[2048,1024]{1,0:T(8,128)(2,1)} async-done(((bf16[64,1024]{1,0:T(8,128)(2,1)}), bf16[2048,1024]{1,0:T(8,128)(2,1)}) %all-gather.13.cloned.1.call-update) | async-done | bytes 4194320 | tf_op jit(solution)/shard_map/all_gather | solution.py:187
  197.8 2.9 fusion.3
  200.9 1.3 collective-permute-start
  202.7 58.4 %all-gather.15.cloned.1.call-done = bf16[1024,2048]{0,1:T(8,128)(2,1)} async-done(((bf16[1024,64]{0,1:T(8,128)(2,1)}), bf16[1024,2048]{0,1:T(8,128)(2,1)}) %all-gather.15.cloned.1.call-update) | async-done | bytes 4194320 | tf_op jit(solution)/shard_map/all_gather | solution.py:283
  261.1 63.2 %all-gather.9.cloned.1.call-done = bf16[2048,1024]{1,0:T(8,128)(2,1)} async-done(((bf16[64,1024]{1,0:T(8,128)(2,1)}), bf16[2048,1024]{1,0:T(8,128)(2,1)}) %all-gather.9.cloned.1.call-update) | async-done | bytes 4194320 | tf_op jit(solution)/shard_map/all_gather | solution.py:185
  324.3 5.8 %fusion.11 = f32[128,2048]{1,0:T(8,128)S(1)} fusion(bf16[1024,2048]{0,1:T(8,128)(2,1)} %all-gather.15.cloned.1.call-done, bf16[2048,1024]{1,0:T(8,128)(2,1)} %all-gather.9.cloned.1.call-done, bf16[128,1024]{1,0:T(8,128)(2,1)S(1)} %fusion.3, bf16[2,1024]{1,0:T(2,128)(2,1)S(1)} %collective-permute-done, f32[128]{0:T(128)S(1)} %get-tuple-element.28, ...), kind=kOutput, calls=%fused_computation.18 | convolution fusion | flops 1077542912 | bytes 10250240 | tf_op jit(solution)/shard_map/dot_general | solution.py:288
  330.2 49.4 %all-gather.21.cloned.1.call-done = f32[64,8,512]{2,1,0:T(8,128)} async-done(((f32[2,8,512]{2,1,0:T(8,128)}), f32[64,8,512]{2,1,0:T(8,128)}) %all-gather.21.cloned.1.call-update) | async-done | bytes 1048592 | tf_op jit(solution)/shard_map/all_gather | solution.py:230
  379.6 2.1 join.1
  381.8 1.3 broadcast_in_dim.24.sre_ref
  383.1 1.3 broadcast_in_dim.25.sim_ref
  384.4 9.0 %mix.1 = bf16[128,1024]{1,0:T(8,128)(2,1)} custom-call(bf16[128,1024]{1,0:T(8,128)(2,1)} %convolution_convert_fusion.u_ref, f32[1024,64]{1,0:T(8,128)} %bitcast.39, f32[1024,64]{1,0:T(8,128)} %bitcast.37, f32[1024,64]{1,0:T(8,128)} %bitcast.41, f32[1024,64]{1,0:T(8,128)} %bitcast.42, f32[8,8,512]{2,1,0:T(8,128)} %get-tuple-element.20.pre_ref, ...), custom_call_target="tpu_custom_call" | custom-call | tf_op jit(solution)/shard_map/mix/pallas_call | solution.py:243
  393.4 49.6 %all-gather.19.cloned.1.call-done = bf16[1024,2048]{0,1:T(8,128)(2,1)} async-done(((bf16[1024,64]{0,1:T(8,128)(2,1)}), bf16[1024,2048]{0,1:T(8,128)(2,1)}) %all-gather.19.cloned.1.call-update) | async-done | bytes 4194320 | tf_op jit(solution)/shard_map/all_gather | solution.py:284
  443.0 4.6 %fusion = bf16[128,2048]{1,0:T(8,128)(2,1)} fusion(f32[128,2048]{1,0:T(8,128)S(1)} %fusion.11, bf16[128,1024]{1,0:T(8,128)(2,1)} %mix.1, bf16[1024,2048]{0,1:T(8,128)(2,1)} %all-gather.19.cloned.1.call-done), kind=kOutput, calls=%fused_computation.1 | convolution fusion | flops 537395200 | bytes 6029312 | tf_op jit(solution)/shard_map/dot_general | solution.py:289
  (43 shorter events, 8.5 us)
Async XLA Ops:
  6.5 64.6 %copy-start = (bf16[128,2048]{1,0:T(8,128)(2,1)S(1)}, bf16[128,2048]{1,0:T(8,128)(2,1)}, u32[]{:S(2)}) copy-start(bf16[128,2048]{1,0:T(8,128)(2,1)} %param.18) | copy-start | bytes 1572868
  6.5 64.6 %all-gather.17.cloned.1.call-start = ((), (), s32[]{:S(2)}) async-start(), calls=%async_computation.4 | async-start | bytes 4325376 | tf_op jit(solution)/shard_map/all_gather | solution.py:188
  7.3 127.2 %all-gather.11.cloned.1.call-start = ((), (), s32[]{:S(2)}) async-start(), calls=%async_computation.1 | async-start | bytes 4325376 | tf_op jit(solution)/shard_map/all_gather | solution.py:186
  8.0 189.8 %all-gather.13.cloned.1.call-start = ((), (), s32[]{:S(2)}) async-start(), calls=%async_computation.2 | async-start | bytes 4325376 | tf_op jit(solution)/shard_map/all_gather | solution.py:187
  8.7 252.3 %all-gather.15.cloned.1.call-start = ((), (), s32[]{:S(2)}) async-start(), calls=%async_computation.3 | async-start | bytes 4325376 | tf_op jit(solution)/shard_map/all_gather | solution.py:283
  9.3 315.0 %all-gather.9.cloned.1.call-start = ((), (), s32[]{:S(2)}) async-start(), calls=%async_computation | async-start | bytes 4325376 | tf_op jit(solution)/shard_map/all_gather | solution.py:185
  9.9 369.7 %all-gather.21.cloned.1.call-start = ((), (), s32[]{:S(2)}) async-start(), calls=%async_computation.6 | async-start | bytes 1081344 | tf_op jit(solution)/shard_map/all_gather | solution.py:230
  61.0 25.1 %copy-start.2 = (s32[128]{0:T(128)S(1)}, s32[128]{0:T(128)}, u32[]{:S(2)}) copy-start(s32[128]{0:T(128)} %param.19) | copy-start | bytes 1540
  61.0 25.8 %copy-start.1 = (bf16[3,1024]{1,0:T(4,128)(2,1)S(1)}, bf16[3,1024]{1,0:T(4,128)(2,1)}, u32[]{:S(2)}) copy-start(bf16[3,1024]{1,0:T(4,128)(2,1)} %param.24) | copy-start | bytes 18436
  84.0 359.0 %all-gather.19.cloned.1.call-start = ((), (), s32[]{:S(2)}) async-start(), calls=%async_computation.5 | async-start | bytes 4325376 | tf_op jit(solution)/shard_map/all_gather | solution.py:284
  200.9 123.5 %collective-permute-start = (bf16[2,1024]{1,0:T(2,128)(2,1)S(1)}, bf16[2,1024]{1,0:T(2,128)(2,1)S(1)}, u32[]{:S(2)}, u32[]{:S(2)}) collective-permute-start(bf16[2,1024]{1,0:T(2,128)(2,1)S(1)} %broadcast_select_fusion), channel_id=1, source_target_pairs={{0,1},{1,2},{2,3},{3,4},{4,5},{5,6},{6,7},{7,8},{8,9},{9,10},{10,1... | collective-permute-start | bytes 12296 | tf_op jit(solution)/shard_map/ppermute | solution.py:23
Sparse Core Ops, SparseCore 0:
  10.2 60.9 all-gather.16
  74.0 60.3 all-gather.10
  137.3 60.4 all-gather.12
  200.5 60.4 all-gather.14
  263.8 60.4 all-gather.8
  327.0 52.5 all-gather.20
  382.5 60.5 all-gather.18

commit v2 on v1

--- a/solution.py
+++ b/solution.py
@@ -181,20 +181,37 @@
         decay_rate, frequency, step_log, input_real, input_imag
     )
     doc_float = documents.astype(jnp.float32)
-    pieces = (
-        lax.all_gather(out_gate_weight, "sp", axis=0, tiled=True),
-        lax.all_gather(in_gate_weight, "sp", axis=0, tiled=True),
-        lax.all_gather(value_weight, "sp", axis=0, tiled=True),
-        lax.all_gather(state_in_weight, "sp", axis=0, tiled=True),
-    )
-    gate_sum, inner_sum, value_sum, driven_sum = tuple(
-        (jnp.dot(normed, piece, preferred_element_type=jnp.float32) for piece in pieces)
-    )
-    driven = driven_sum.astype(jnp.bfloat16)
+    devices = lax.axis_size("sp")
+    near = math.gcd(devices, 4)
+    rows_of = [[i * near + j for j in range(near)] for i in range(devices // near)]
+    columns_of = [[i * near + j for i in range(devices // near)] for j in range(near)]
+    weights = (out_gate_weight, in_gate_weight, value_weight, state_in_weight)
+    strip = out_gate_weight.shape[1] // near
+    strips = jnp.stack(
+        [
+            jnp.concatenate([w[:, j * strip : (j + 1) * strip] for w in weights], axis=1)
+            for j in range(near)
+        ]
+    )
+    strips = lax.all_to_all(strips, "sp", 0, 0, axis_index_groups=rows_of, tiled=True)
+    strips = lax.all_gather(
+        strips.reshape(-1, len(weights) * strip),
+        "sp",
+        axis=0,
+        axis_index_groups=columns_of,
+        tiled=True,
+    )
+    near_rows = lax.all_gather(normed, "sp", axis=0, axis_index_groups=rows_of, tiled=True)
+    sums = jnp.dot(near_rows, strips, preferred_element_type=jnp.float32).astype(jnp.bfloat16)
+    sums = lax.all_to_all(
+        sums.reshape(near, row_count, -1), "sp", 0, 0, axis_index_groups=rows_of, tiled=True
+    )
+    gate_sum, inner_sum, value_sum, driven = (
+        jnp.concatenate([sums[j, :, k * strip : (k + 1) * strip] for j in range(near)], axis=1)
+        for k in range(len(weights))
+    )
     place = lax.axis_index("sp")
-    devices = lax.axis_size("sp")
-    lasts = lax.all_gather(doc_float[-1], "sp")
-    in_last = jnp.where(place > 0, lasts[jnp.maximum(place - 1, 0)], -1.0)
+    in_last = jnp.where(place > 0, from_behind(doc_float[-1:], "sp", 1)[0], -1.0)
     lanes = math.gcd(groups * group_size, 128)
     blocks = groups * group_size // lanes
     span = lanes // group_size * state_size
@@ -227,7 +244,14 @@
         out_shape=[state_shape] * 2,
         name="ends",
     )(driven, b_re, b_im, pow_re, pow_im, masks)
-    ends = lax.all_gather(jnp.stack([e.reshape(blocks, span) for e in ends]), "sp")
+    packed = jnp.concatenate(
+        [e.reshape(blocks, span) for e in ends] + [jnp.broadcast_to(doc_float[-1], (1, span))]
+    )
+    packed = lax.all_gather(packed, "sp", axis_index_groups=rows_of)
+    packed = lax.all_gather(packed, "sp", axis_index_groups=columns_of)
+    packed = packed.reshape(devices, 2 * blocks + 1, span)
+    ends = packed[:, : 2 * blocks].reshape(devices, 2, blocks, span)
+    lasts = packed[:, 2 * blocks, 0]
     source = jnp.arange(devices)
     take = ((source < place) & (lasts == in_last)).astype(jnp.float32)
     later = (source >= place).astype(jnp.float32)
@@ -279,19 +303,19 @@
             * same_doc[:, None]
         )
     conv_out = (out_gate * total).astype(jnp.bfloat16)
-    conv_columns, state_columns = (
-        lax.all_gather(conv_out_weight, "sp", axis=1, tiled=True),
-        lax.all_gather(state_out_weight, "sp", axis=1, tiled=True),
-    )
-    return lax.psum_scatter(
-        (
-            jnp.dot(conv_out, conv_columns, preferred_element_type=jnp.float32)
-            + jnp.dot(ssm_out, state_columns, preferred_element_type=jnp.float32)
-        ).astype(jnp.bfloat16),
-        "tp",
-        scatter_dimension=0,
-        tiled=True,
-    )
+    columns = jnp.concatenate([conv_out_weight, state_out_weight], axis=0).T
+    columns = lax.all_gather(columns, "sp", axis=0, axis_index_groups=columns_of, tiled=True)
+    mixers = jnp.concatenate([conv_out, ssm_out], axis=1)
+    mixers = lax.all_gather(mixers, "sp", axis=0, axis_index_groups=rows_of, tiled=True)
+    part = lax.dot_general(
+        mixers, columns, (((1,), (1,)), ((), ())), preferred_element_type=jnp.float32
+    ).astype(jnp.bfloat16)
+    part = lax.all_to_all(
+        part.reshape(near, row_count, -1), "sp", 0, 0, axis_index_groups=rows_of, tiled=True
+    )
+    part = part.reshape(near, row_count, devices // near, -1)
+    part = part.transpose(1, 2, 0, 3).reshape(row_count, -1)
+    return lax.psum_scatter(part, "tp", scatter_dimension=0, tiled=True)
 
 
 def solution(mesh):

time: 460 us -> 291 us (0.63)
  waiting for transfers between devices: 341 us -> 181 us
  matrix products: 19.9 us -> 9.62 us
  blocking collectives: 38.3 us -> 28.9 us
  starting transfers between devices: 1.52 us -> 7.28 us
    all_gather x7 -> x5, waiting for transfers between devices: 337 us -> 173 us  [the longest x1 73.1 us: shards(): lax.all_gather(strips.reshape(-1, len(weights) * strip), 'sp', axis=0, ax...]
    unnamed x1 -> x0, blocking collectives: 38.3 us -> none
    all_to_all x0 -> x2, blocking collectives: none -> 22.4 us  [the longest x1 11.7 us: shards(): lax.all_to_all(strips, 'sp', 0, 0, axis_index_groups=rows_of, tiled=True)]
    dot_general x5 -> x2, matrix products: 19.9 us -> 9.62 us  [the longest x1 6.12 us: shards(): jnp.dot(near_rows, strips, preferred_element_type=jnp.float32)]
    all_gather x0 -> x1, blocking collectives: none -> 6.47 us  [shards(): packed = lax.all_gather(packed, 'sp', axis_index_groups=rows_of)]
    all_to_all x0 -> x1, waiting for transfers between devices: none -> 6.32 us  [shards(): lax.all_to_all(sums.reshape(near, row_count, -1), 'sp', 0, 0, axis_index_...]
  transfers between devices with their start and end apart: 8 -> 8, of which waited for: 7 -> 7; matrix products, arithmetic and copies ran while one was open for 8% -> 9% of each run, Pallas kernels for 4% -> 4%
where the time goes in v2:
time: 291 us; the launch traced here: 286 us
  waiting for transfers between devices  181 us (62%)
  blocking collectives  28.9 us (10%)
  Pallas kernels  19 us (7%)
  other arithmetic  16.1 us (6%)
  between operations  14.1 us (5%)
  local copies, waits for them, and re-layouts  10.7 us (4%)
  matrix products  9.62 us (3%)
  starting transfers between devices  7.28 us (3%)
    all_gather x1, waiting for transfers between devices, shards(): lax.all_gather(strips.reshape(-1, len(weights) * strip), 'sp', axis=0, ax...  73.1 us
    all_gather x1, waiting for transfers between devices, shards(): packed = lax.all_gather(packed, 'sp', axis_index_groups=columns_of)  36 us
    all_gather x1, waiting for transfers between devices, shards(): lax.all_gather(columns, 'sp', axis=0, axis_index_groups=columns_of, tiled...  29.5 us
    all_gather x1, waiting for transfers between devices, shards(): lax.all_gather(mixers, 'sp', axis=0, axis_index_groups=rows_of, tiled=True)  25 us
    all_to_all x1, blocking collectives, shards(): lax.all_to_all(strips, 'sp', 0, 0, axis_index_groups=rows_of, tiled=True)  11.7 us
    all_to_all x1, blocking collectives, shards(): lax.all_to_all(part.reshape(near, row_count, -1), 'sp', 0, 0, axis_index_...  10.7 us
    all_gather x1, waiting for transfers between devices, shards(): lax.all_gather(normed, 'sp', axis=0, axis_index_groups=rows_of, tiled=True)  9.55 us
    pallas_call x1, Pallas kernels, shards(): pl.pallas_call(functools.partial(mix_body, group_size), grid=(blocks,), i...  9 us
  transfers between devices with their start and end apart: 8, of which 7 were waited for; matrix products, arithmetic and copies ran while one was open for 9% of the time, Pallas kernels for 4%

profile of v2, /device:TPU:31, one launch (start us, length us, event | category | flops | bytes accessed | tf_op | source)
XLA Modules:
  0.0 286.4 jit_solution(1781232793749191049)
XLA Ops:
  6.6 0.8 convert_element_type.67
  7.3 1.2 fusion
  8.6 2.0 fusion.2
  11.0 11.7 %all_to_all.15 = bf16[4,64,1024]{2,1,0:T(8,128)(2,1)} all-to-all(bf16[4,64,1024]{2,1,0:T(8,128)(2,1)S(1)} %pad_maximum_fusion), channel_id=1, replica_groups={{0,1,2,3},{4,5,6,7},{8,9,10,11},{12,13,14,15},{16,17,18,19},{20,21,22,2..., dimensions={0} | all-to-all | bytes 1048576 | tf_op jit(solution)/shard_map/all_to_all | solution.py:196
  23.4 1.3 collective-permute-start.1
  25.3 9.5 %all-gather.9.cloned.1.call-done = bf16[512,2048]{1,0:T(8,128)(2,1)} async-done(((bf16[128,2048]{1,0:T(8,128)(2,1)}), bf16[512,2048]{1,0:T(8,128)(2,1)}) %all-gather.9.cloned.1.call-update) | async-done | bytes 2097168 | tf_op jit(solution)/shard_map/all_gather | solution.py:204
  34.9 73.1 %all-gather.11.cloned.1.call-done = bf16[2048,1024]{1,0:T(8,128)(2,1)} async-done(((bf16[256,1024]{1,0:T(8,128)(2,1)}), bf16[2048,1024]{1,0:T(8,128)(2,1)}) %all-gather.11.cloned.1.call-update) | async-done | bytes 4194320 | tf_op jit(solution)/shard_map/all_gather | solution.py:197
  108.0 6.1 %convolution_convert_fusion = bf16[512,1024]{1,0:T(8,128)(2,1)} fusion(bf16[512,2048]{1,0:T(8,128)(2,1)} %all-gather.9.cloned.1.call-done, bf16[2048,1024]{1,0:T(8,128)(2,1)} %all-gather.11.cloned.1.call-done), kind=kOutput, calls=%fused_computation | convolution fusion | flops 2148007936 | bytes 7340032 | tf_op jit(solution)/shard_map/dot_general | solution.py:205
  114.1 4.6 %all-to-all-start.1 = ((bf16[4,128,1024]{2,1,0:T(8,128)(2,1)}), bf16[4,128,1024]{2,1,0:T(8,128)(2,1)S(1)}, u32[]{:S(2)}, u32[]{:S(2)}) async-start(bf16[4,128,1024]{2,1,0:T(8,128)(2,1)} %bitcast.5), calls=%async_computation.1 | async-start | bytes 2097152 | tf_op jit(solution)/shard_map/all_to_all | solution.py:206
  118.7 1.3 fusion.5
  121.5 1.1 multiply_add_fusion
  124.9 6.3 %all-to-all-done.1 = bf16[4,128,1024]{2,1,0:T(8,128)(2,1)S(1)} async-done(((bf16[4,128,1024]{2,1,0:T(8,128)(2,1)}), bf16[4,128,1024]{2,1,0:T(8,128)(2,1)S(1)}, u32[]{:S(2)}, u32[]{:S(2)}) %all-to-all-start.1) | async-done | bytes 1048608 | tf_op jit(solution)/shard_map/all_to_all | solution.py:206
  131.4 0.7 pad_maximum_fusion.3.u_ref
  132.1 7.8 %ends.1 = (f32[8,1,512]{2,1,0:T(1,128)}, f32[8,1,512]{2,1,0:T(1,128)}) custom-call(bf16[128,1024]{1,0:T(8,128)(2,1)} %pad_maximum_fusion.3.u_ref, f32[1024,64]{1,0:T(8,128)} %bitcast.92, f32[1024,64]{1,0:T(8,128)} %bitcast.90, f32[8,8,512]{2,1,0:T(8,128)} %get-tuple-element.52.pre_ref, f32[8,8,512]{2,1,0:T(8,128)} %get-tuple-element.51.pim_ref, ...), custom_call_target="tpu_custom_call" | custom-call | tf_op jit(solution)/shard_map/ends/pallas_call | solution.py:239
  139.9 0.7 copy.39
  140.6 0.7 copy.40
  141.4 6.5 %all-gather.2 = f32[4,17,512]{2,1,0:T(8,128)} all-gather(f32[1,17,512]{2,1,0:T(8,128)S(1)} %maximum_bitcast_fusion.5), channel_id=2, replica_groups={{0,1,2,3},{4,5,6,7},{8,9,10,11},{12,13,14,15},{16,17,18,19},{20,21,22,2..., dimensions={0}, use_global_device_ids=true | all-gather | bytes 174080 | tf_op jit(solution)/shard_map/all_gather | solution.py:250
  150.3 1.3 collective-permute-start
  152.1 1.2 collective-permute-done
  153.7 36.0 %all-gather.17.cloned.1.call-done = f32[32,17,512]{2,1,0:T(8,128)} async-done(((f32[4,17,512]{2,1,0:T(8,128)}), f32[32,17,512]{2,1,0:T(8,128)}) %all-gather.17.cloned.1.call-update) | async-done | bytes 1114128 | tf_op jit(solution)/shard_map/all_gather | solution.py:251
  189.7 1.6 compare_reduce_fusion
  191.9 2.3 slice_bitcast_fusion.end_ref
  194.2 2.2 join.1
  196.4 1.3 broadcast_in_dim.27.sre_ref
  197.7 1.3 broadcast_in_dim.28.sim_ref
  199.1 9.0 %mix.1 = bf16[128,1024]{1,0:T(8,128)(2,1)} custom-call(bf16[128,1024]{1,0:T(8,128)(2,1)} %pad_maximum_fusion.3.u_ref, f32[1024,64]{1,0:T(8,128)} %bitcast.93, f32[1024,64]{1,0:T(8,128)} %bitcast.91, f32[1024,64]{1,0:T(8,128)} %bitcast.98, f32[1024,64]{1,0:T(8,128)} %bitcast.99, f32[8,8,512]{2,1,0:T(8,128)} %get-tuple-element.52.pre_ref, ...), custom_call_target="tpu_custom_call" | custom-call | tf_op jit(solution)/shard_map/mix/pallas_call | solution.py:267
  208.0 1.8 pad_maximum_fusion.1
  209.9 29.5 %all-gather.15.cloned.1.call-done = bf16[512,2048]{1,0:T(8,128)(2,1)} async-done(((bf16[64,2048]{1,0:T(8,128)(2,1)}), bf16[512,2048]{1,0:T(8,128)(2,1)}) %all-gather.15.cloned.1.call-update) | async-done | bytes 2097168 | tf_op jit(solution)/shard_map/all_gather | solution.py:307
  239.4 25.0 %all-gather.13.cloned.1.call-done = bf16[512,2048]{1,0:T(8,128)(2,1)} async-done(((bf16[128,2048]{1,0:T(8,128)(2,1)}), bf16[512,2048]{1,0:T(8,128)(2,1)}) %all-gather.13.cloned.1.call-update) | async-done | bytes 2097168 | tf_op jit(solution)/shard_map/all_gather | solution.py:309
  264.3 3.5 %convolution_convert_fusion.1 = bf16[512,512]{1,0:T(8,128)(2,1)S(1)} fusion(bf16[512,2048]{1,0:T(8,128)(2,1)} %all-gather.13.cloned.1.call-done, bf16[512,2048]{1,0:T(8,128)(2,1)} %all-gather.15.cloned.1.call-done), kind=kOutput, calls=%fused_computation.3 | convolution fusion | flops 1074003968 | bytes 4718592 | tf_op jit(solution)/shard_map/dot_general | solution.py:310
  268.1 10.7 %all_to_all.16 = bf16[4,128,512]{1,2,0:T(8,128)(2,1)S(1)} all-to-all(bf16[4,128,512]{1,2,0:T(8,128)(2,1)S(1)} %copy.32), channel_id=1, replica_groups={{0,1,2,3},{4,5,6,7},{8,9,10,11},{12,13,14,15},{16,17,18,19},{20,21,22,2..., dimensions={0} | all-to-all | bytes 1048576 | tf_op jit(solution)/shard_map/all_to_all | solution.py:313
  278.9 1.0 copy.34
  (79 shorter events, 9.1 us)
Async XLA Ops:
  6.5 4.2 %copy-start.2 = (bf16[64,1024]{1,0:T(8,128)(2,1)S(1)}, bf16[64,1024]{1,0:T(8,128)(2,1)}, u32[]{:S(2)}) copy-start(bf16[64,1024]{1,0:T(8,128)(2,1)} %param.21) | copy-start | bytes 393220
  6.5 4.2 %copy-start.3 = (bf16[64,1024]{1,0:T(8,128)(2,1)S(1)}, bf16[64,1024]{1,0:T(8,128)(2,1)}, u32[]{:S(2)}) copy-start(bf16[64,1024]{1,0:T(8,128)(2,1)} %param.22) | copy-start | bytes 393220
  6.5 4.2 %copy-start.4 = (bf16[64,1024]{1,0:T(8,128)(2,1)S(1)}, bf16[64,1024]{1,0:T(8,128)(2,1)}, u32[]{:S(2)}) copy-start(bf16[64,1024]{1,0:T(8,128)(2,1)} %param.23) | copy-start | bytes 393220
  6.5 4.3 %copy-start.5 = (bf16[64,1024]{1,0:T(8,128)(2,1)S(1)}, bf16[64,1024]{1,0:T(8,128)(2,1)}, u32[]{:S(2)}) copy-start(bf16[64,1024]{1,0:T(8,128)(2,1)} %param.25) | copy-start | bytes 393220
  6.5 28.3 %all-gather.9.cloned.1.call-start = ((), (), s32[]{:S(2)}) async-start(), calls=%async_computation.3 | async-start | bytes 2621440 | tf_op jit(solution)/shard_map/all_gather | solution.py:204
  10.6 97.4 %all-gather.11.cloned.1.call-start = ((), (), s32[]{:S(2)}) async-start(), calls=%async_computation.4 | async-start | bytes 4718592 | tf_op jit(solution)/shard_map/all_gather | solution.py:197
  10.8 11.9 %copy-start.11 = (s32[128]{0:T(128)S(1)}, s32[128]{0:T(128)}, u32[]{:S(2)}) copy-start(s32[128]{0:T(128)} %param.19) | copy-start | bytes 1540
  10.8 13.9 %copy-start.12 = (f32[64]{0:T(128)S(1)}, f32[64]{0:T(128)}, u32[]{:S(2)}) copy-start(f32[64]{0:T(128)} %param.28) | copy-start | bytes 772
  10.8 13.9 %copy-start.8 = (f32[64,64]{1,0:T(8,128)S(1)}, f32[64,64]{1,0:T(8,128)}, u32[]{:S(2)}) copy-start(f32[64,64]{1,0:T(8,128)} %param.27) | copy-start | bytes 49156
  10.8 13.9 %copy-start.9 = (f32[64,64]{1,0:T(8,128)S(1)}, f32[64,64]{1,0:T(8,128)}, u32[]{:S(2)}) copy-start(f32[64,64]{1,0:T(8,128)} %param.26) | copy-start | bytes 49156
  23.4 99.3 %collective-permute-start.1 = (f32[1]{0:T(128)}, f32[1]{0:T(128)}, u32[]{:S(2)}, u32[]{:S(2)}) collective-permute-start(f32[1]{0:T(128)} %slice.192), channel_id=1, source_target_pairs={{0,1},{1,2},{2,3},{3,4},{4,5},{5,6},{6,7},{7,8},{8,9},{9,10},{10,1... | collective-permute-start | bytes 20 | tf_op jit(solution)/shard_map/ppermute | solution.py:23
  114.1 7.4 %copy-start = (f32[64,64,16]{1,2,0:T(8,128)S(1)}, f32[64,64,16]{1,2,0:T(8,128)}, u32[]{:S(2)}) copy-start(f32[64,64,16]{1,2,0:T(8,128)} %param.29) | copy-start | bytes 786436
  114.1 7.4 %copy-start.1 = (f32[64,64,16]{1,2,0:T(8,128)S(1)}, f32[64,64,16]{1,2,0:T(8,128)}, u32[]{:S(2)}) copy-start(f32[64,64,16]{1,2,0:T(8,128)} %param.30) | copy-start | bytes 786436
  114.1 17.1 %all-to-all-start.1 = ((bf16[4,128,1024]{2,1,0:T(8,128)(2,1)}), bf16[4,128,1024]{2,1,0:T(8,128)(2,1)S(1)}, u32[]{:S(2)}, u32[]{:S(2)}) async-start(bf16[4,128,1024]{2,1,0:T(8,128)(2,1)} %bitcast.5), calls=%async_computation.1 | async-start | bytes 2097152 | tf_op jit(solution)/shard_map/all_to_all | solution.py:206
  118.7 71.1 %all-gather.17.cloned.1.call-start = ((), (), s32[]{:S(2)}) async-start(), calls=%async_computation.7 | async-start | bytes 1769472 | tf_op jit(solution)/shard_map/all_gather | solution.py:251
  124.9 23.0 %copy-start.6 = (bf16[1024,64]{0,1:T(8,128)(2,1)S(1)}, bf16[1024,64]{0,1:T(8,128)(2,1)}, u32[]{:S(2)}) copy-start(bf16[1024,64]{0,1:T(8,128)(2,1)} %param.35) | copy-start | bytes 393220
  124.9 23.0 %copy-start.7 = (bf16[1024,64]{0,1:T(8,128)(2,1)S(1)}, bf16[1024,64]{0,1:T(8,128)(2,1)}, u32[]{:S(2)}) copy-start(bf16[1024,64]{0,1:T(8,128)(2,1)} %param.34) | copy-start | bytes 393220
  131.4 18.8 %copy-start.10 = (bf16[3,1024]{1,0:T(4,128)(2,1)S(1)}, bf16[3,1024]{1,0:T(4,128)(2,1)}, u32[]{:S(2)}) copy-start(bf16[3,1024]{1,0:T(4,128)(2,1)} %param.24) | copy-start | bytes 18436
  147.9 91.4 %all-gather.15.cloned.1.call-start = ((), (), s32[]{:S(2)}) async-start(), calls=%async_computation.6 | async-start | bytes 2359296 | tf_op jit(solution)/shard_map/all_gather | solution.py:307
  148.7 115.6 %all-gather.13.cloned.1.call-start = ((), (), s32[]{:S(2)}) async-start(), calls=%async_computation.5 | async-start | bytes 2621440 | tf_op jit(solution)/shard_map/all_gather | solution.py:309
  150.3 3.0 %collective-permute-start = (bf16[2,1024]{1,0:T(2,128)(2,1)S(1)}, bf16[2,1024]{1,0:T(2,128)(2,1)S(1)}, u32[]{:S(2)}, u32[]{:S(2)}) collective-permute-start(bf16[2,1024]{1,0:T(2,128)(2,1)S(1)} %broadcast_select_fusion), channel_id=1, source_target_pairs={{0,1},{1,2},{2,3},{3,4},{4,5},{5,6},{6,7},{7,8},{8,9},{9,10},{10,1... | collective-permute-start | bytes 12296 | tf_op jit(solution)/shard_map/ppermute | solution.py:23
Sparse Core Ops, SparseCore 0:
  10.8 24.0 all-gather.8
  37.0 70.9 all-gather.10
  148.0 41.6 all-gather.16
  191.7 47.5 all-gather.14
  240.8 23.5 all-gather.12
